TPU v7x, 32 devices: a whole 2x2x4 slice. The times are simulated.
32 devices in a mesh: sp: 16 (over z, y, x), dp: 2 (over core).
Axes of the slice: x: 2, y: 2, z: 4, core: 2. Of those that a mesh axis runs over, the one named last changes fastest.
Arguments:
- inputs: bfloat16 [2, 2048, 2048], P('dp', 'sp'), may hold values from -6 to 6
- w_key: bfloat16 [2048, 256], P('dp')
- w_value: bfloat16 [2048, 256], P('dp'), may hold values from -0.125 to 0.125
- queries: bfloat16 [2, 2048, 2048], P('dp', 'sp')
- cotangent: bfloat16 [2, 2048, 2048], P('dp', 'sp'), may hold values from -6 to 6
- cum_gate: float32 [2, 32, 2048], P('dp', 'sp'), as said below
Outputs:
- grad_input: bfloat16 [2, 2048, 2048], P('dp', 'sp')
- grad_queries: bfloat16 [2, 2048, 2048], P('dp', 'sp')
- grad_cum: float32 [2, 32, 2048], P('dp', 'sp')
- grad_w_key: float32 [2048, 256], P('dp')
- grad_w_value: float32 [2048, 256], P('dp')
Inputs may be any that keep to these rules, and one draw needn't show every extreme that they name: Along each sequence cum_gate never rises, and it is at most zero.
All inputs are finite; a program needn't handle non-finite values.
Results may differ from a plain program's by a relative error of at most 0.023.
Values may be sent and summed in bfloat16 or wider, within the bound.
A program may use at most 128 MiB of HBM per device.

v0:
```python
import functools

import jax
import jax.numpy as jnp
from jax import lax
from jax.experimental import pallas as pl
from jax.experimental.pallas import tpu as pltpu
from jax.sharding import PartitionSpec as P

HD = 64
LANES = 128
LOG2E = 1.4426950408889634
MESH = pl.DeviceIdType.MESH
VMEM = pl.BlockSpec(memory_space=pltpu.VMEM)
BF16 = jnp.bfloat16
F32 = jnp.float32


def dot_nn(a, b):
    return jnp.dot(a, b, preferred_element_type=F32)


def dot_nt(a, b):
    return lax.dot_general(a, b, (((1,), (1,)), ((), ())), preferred_element_type=F32)


def dot_tn(a, b):
    return lax.dot_general(a, b, (((0,), (0,)), ((), ())), preferred_element_type=F32)


def greet(n, m):
    me, mine = lax.axis_index("sp"), lax.axis_index("dp")
    barrier = pltpu.get_barrier_semaphore()

    @pl.loop(1, n)
    def _(k):
        pl.semaphore_signal(
            barrier, inc=1, device_id={"sp": lax.rem(me + k, n)}, device_id_type=MESH
        )

    @pl.loop(1, m)
    def _(k):
        pl.semaphore_signal(
            barrier, inc=1, device_id={"dp": lax.rem(mine + k, m)}, device_id_type=MESH
        )

    pl.semaphore_wait(barrier, n + m - 2)


def start_all(n, make):
    @pl.loop(1, n)
    def _(k):
        make(k).start()


def wait_all(n, make):
    @pl.loop(1, n)
    def _(k):
        make(k).wait()


def remote(src, dst, sems, k, device):
    return pltpu.make_async_remote_copy(
        src_ref=src,
        dst_ref=dst,
        send_sem=sems.at[0, k],
        recv_sem=sems.at[1, k],
        device_id=device,
        device_id_type=MESH,
    )


def column_block(ref, j, width):
    if len(ref.shape) == 3:
        return ref.at[j]
    return ref.at[:, pl.ds(pl.multiple_of(j * width, LANES), width)]


def row_block(ref, j, rows):
    return ref.at[pl.ds(pl.multiple_of(j * rows, 16), rows)]


def gather_kernel(
    n, m, width, kv_heads,
    q_ref, g_ref, x_ref, wk_ref, wv_ref,
    q_out, g_out, kv_out, w_out, x_out,
    kv_block, q_sems, g_sems, kv_sems, wk_sems, wv_sems, x_sems, own_sems,
):
    me, mine = lax.axis_index("sp"), lax.axis_index("dp")
    positions = x_ref.shape[0]
    rows, kv_width = wk_ref.shape
    greet(n, m)

    def target(k):
        return lax.rem(me + k, n)

    def peer(k):
        return lax.rem(mine + k, m)

    def wk_copy(k):
        dst = row_block(w_out, mine, rows).at[:, pl.ds(0, kv_width)]
        return remote(wk_ref, dst, wk_sems, k, {"dp": peer(k)})

    def wv_copy(k):
        dst = row_block(w_out, mine, rows).at[:, pl.ds(kv_width, kv_width)]
        return remote(wv_ref, dst, wv_sems, k, {"dp": peer(k)})

    def x_copy(k):
        return remote(
            column_block(x_ref, peer(k), rows), x_out.at[mine], x_sems, k, {"dp": peer(k)}
        )

    def q_copy(k):
        return remote(
            column_block(q_ref, target(k), width),
            row_block(q_out, me, positions), q_sems, k, {"sp": target(k)},
        )

    def g_copy(k):
        return remote(
            column_block(g_ref, target(k), width),
            row_block(g_out, me, positions), g_sems, k, {"sp": target(k)},
        )

    def kv_copy(k):
        group = (target(k) * kv_heads) // n
        return remote(
            column_block(kv_block, group, 2 * HD),
            row_block(kv_out, me, positions), kv_sems, k, {"sp": target(k)},
        )

    own = [
        pltpu.make_async_copy(
            wk_ref, row_block(w_out, mine, rows).at[:, pl.ds(0, kv_width)], own_sems.at[0]
        ),
        pltpu.make_async_copy(
            wv_ref, row_block(w_out, mine, rows).at[:, pl.ds(kv_width, kv_width)], own_sems.at[1]
        ),
        pltpu.make_async_copy(column_block(x_ref, mine, rows), x_out.at[mine], own_sems.at[2]),
        pltpu.make_async_copy(
            column_block(q_ref, me, width), row_block(q_out, me, positions), own_sems.at[3]
        ),
        pltpu.make_async_copy(
            column_block(g_ref, me, width), row_block(g_out, me, positions), own_sems.at[4]
        ),
    ]
    start_all(m, wk_copy)
    start_all(m, wv_copy)
    start_all(n, q_copy)
    start_all(n, g_copy)
    for copy in own:
        copy.start()
    wait_all(m, wk_copy)
    wait_all(m, wv_copy)
    start_all(m, x_copy)
    for copy in own:
        copy.wait()
    both = dot_nn(x_ref[...], w_out[...]).astype(BF16)
    pieces = []
    for group in range(kv_heads):
        pieces.append(both[:, group * HD : (group + 1) * HD])
        pieces.append(both[:, kv_width + group * HD : kv_width + (group + 1) * HD])
    kv_block[...] = jnp.concatenate(pieces, axis=1)
    start_all(n, kv_copy)
    kv_own = pltpu.make_async_copy(
        column_block(kv_block, (me * kv_heads) // n, 2 * HD),
        row_block(kv_out, me, positions), own_sems.at[5],
    )
    kv_own.start()
    kv_own.wait()
    wait_all(m, x_copy)
    wait_all(n, q_copy)
    wait_all(n, g_copy)
    wait_all(n, kv_copy)


def attend_kernel(
    heads, tile,
    q_ref, g_ref, kv_ref, gate_q, gate_k,
    dq_ref, dkv_ref, gc_ref,
    kx, kt, vs, qx, qd, gh, s_buf, d_buf, dk_acc, dv_acc,
):
    length = kv_ref.shape[0]
    scale = HD ** (-0.5)
    keys = kv_ref[:, :HD]
    kt[...] = keys.astype(F32).T.astype(BF16)
    vs[...] = kv_ref[:, HD:]
    dk_acc[...] = jnp.zeros_like(dk_acc)
    dv_acc[...] = jnp.zeros_like(dv_acc)
    lane = lax.broadcasted_iota(jnp.int32, (length, HD), 1)
    for h in range(heads):
        q_head = q_ref[:, h * HD : (h + 1) * HD]
        kx[h] = jnp.concatenate([keys, gate_k[h]], axis=1)
        qx[h] = jnp.concatenate([q_head * jnp.asarray(scale, BF16), gate_q[h]], axis=1)
        mark = jnp.where(lane == h, 1.0, 0.0).astype(BF16)
        qd[h] = jnp.concatenate([q_head, mark], axis=1)
        gh[h] = g_ref[:, h * HD : (h + 1) * HD]
    later = lax.broadcasted_iota(jnp.int32, (tile, tile), 0) > lax.broadcasted_iota(
        jnp.int32, (tile, tile), 1
    )
    every = range(heads)

    def fold(op, a):
        return op(a.reshape(tile // 8, 8, tile), axis=0)

    @pl.loop(0, length // tile)
    def _(i):
        here = pl.ds(pl.multiple_of(i * tile, tile), tile)

        def score(c, tops, diagonal):
            at = pl.ds(pl.multiple_of(c * tile, tile), tile)
            out = []
            for h in every:
                s = dot_nt(kx[h, at, :], qx[h, here, :])
                if diagonal:
                    s = jnp.where(later, -jnp.inf, s)
                s_buf[h, at, :] = s
                out.append(jnp.maximum(tops[h], fold(jnp.max, s)))
            return tuple(out)

        tops = tuple(jnp.full((8, tile), -jnp.inf, F32) for _ in every)
        tops = lax.fori_loop(0, i, lambda c, v: score(c, v, False), tops)
        tops = score(i, tops, True)
        tops = [jnp.max(top, axis=0, keepdims=True) for top in tops]

        def weigh(c, carry):
            at = pl.ds(pl.multiple_of(c * tile, tile), tile)
            out = []
            for h in every:
                total, dots = carry[h]
                d = dot_nt(vs[at, :], gh[h, here, :])
                e = jnp.exp2((s_buf[h, at, :] - tops[h]) * LOG2E)
                s_buf[h, at, :] = e
                d_buf[h, at, :] = d
                out.append((total + fold(jnp.sum, e), dots + fold(jnp.sum, e * d)))
            return tuple(out)

        zero = jnp.zeros((8, tile), F32)
        sums = lax.fori_loop(0, i + 1, weigh, tuple((zero, zero) for _ in every))
        inverse, row_dot = [], []
        for h in every:
            total = jnp.sum(sums[h][0], axis=0, keepdims=True)
            dots = jnp.sum(sums[h][1], axis=0, keepdims=True)
            inv = 1.0 / total
            inverse.append(inv)
            row_dot.append(dots * inv)
            gc_ref[h : h + 1, here] = dots * inv - row_dot[h] * (total * inv)

        def spread(c, carry):
            at = pl.ds(pl.multiple_of(c * tile, tile), tile)
            out = []
            dk = dk_acc[at, :]
            dv = dv_acc[at, :]
            for h in every:
                p = s_buf[h, at, :] * inverse[h]
                low = (p * (d_buf[h, at, :] - row_dot[h])).astype(BF16)
                dv = dv + dot_nn(p.astype(BF16), gh[h, here, :])
                dk = dk + dot_nn(low, qd[h, here, :])
                out.append(carry[h] + dot_nn(kt[:, at], low))
            dk_acc[at, :] = dk
            dv_acc[at, :] = dv
            return tuple(out)

        start = tuple(jnp.zeros((HD, tile), F32) for _ in every)
        grads = lax.fori_loop(0, i + 1, spread, start)
        dq_ref[here, :] = jnp.concatenate([(gr.T * scale) for gr in grads], axis=1).astype(BF16)

    dk = dk_acc[...]
    dkv_ref[...] = jnp.concatenate([dk[:, :HD] * scale, dv_acc[...]], axis=1).astype(BF16)
    columns = dk.T
    gc_ref[...] = gc_ref[...] - columns[HD : HD + heads, :]


def return_kernel(
    n, m, width, kv_heads, reduce_here,
    dq_ref, dkv_ref, x_ref, w_ref,
    gq_out, gx_out, *rest,
):
    if reduce_here:
        (gwk_out, gwv_out, slots, gkv_all, share, parts, mean_block, whole,
         q_sems, kv_sems, gkv_sems, own_sems, rs_sems, ag_sems) = rest
    else:
        share, slots, gkv_all, q_sems, kv_sems, gkv_sems, own_sems = rest
    me, mine = lax.axis_index("sp"), lax.axis_index("dp")
    positions = slots.shape[1]
    kv_width = kv_heads * HD
    greet(n, m)

    def target(k):
        return lax.rem(me + k, n)

    def peer(k):
        return lax.rem(mine + k, m)

    def q_copy(k):
        return remote(
            row_block(dq_ref, target(k), positions),
            column_block(gq_out, me, width), q_sems, k, {"sp": target(k)},
        )

    def kv_copy(k):
        return remote(
            row_block(dkv_ref, target(k), positions), slots.at[me], kv_sems, k,
            {"sp": target(k)},
        )

    def gkv_copy(k):
        return remote(gkv_all.at[mine], gkv_all.at[mine], gkv_sems, k, {"dp": peer(k)})

    start_all(n, kv_copy)
    start_all(n, q_copy)
    kv_own = pltpu.make_async_copy(
        row_block(dkv_ref, me, positions), slots.at[me], own_sems.at[0]
    )
    q_own = pltpu.make_async_copy(
        row_block(dq_ref, me, positions), column_block(gq_out, me, width), own_sems.at[1]
    )
    kv_own.start()
    q_own.start()
    kv_own.wait()
    q_own.wait()
    wait_all(n, kv_copy)
    per = n // kv_heads
    groups = []
    for group in range(kv_heads):
        total = slots[group * per].astype(F32)
        for j in range(1, per):
            total = total + slots[group * per + j].astype(F32)
        groups.append(total)
    gkv = jnp.concatenate(
        [total[:, :HD] for total in groups] + [total[:, HD:] for total in groups], axis=1
    ).astype(BF16)
    gkv_all[mine] = gkv
    start_all(m, gkv_copy)
    gx_out[...] = dot_nt(gkv, w_ref[...]).astype(BF16)
    wait_all(m, gkv_copy)
    total = dot_tn(x_ref[0], gkv_all[0])
    for j in range(1, m):
        total = total + dot_tn(x_ref[j], gkv_all[j])
    share[...] = total.astype(BF16)
    if reduce_here:
        piece = share.shape[0] // n

        def rs_copy(k):
            return remote(
                row_block(share, target(k), piece), parts.at[me], rs_sems, k,
                {"sp": target(k)},
            )

        def ag_copy(k):
            return remote(
                mean_block, row_block(whole, me, piece), ag_sems, k, {"sp": target(k)}
            )

        start_all(n, rs_copy)
        rs_own = pltpu.make_async_copy(row_block(share, me, piece), parts.at[me], own_sems.at[2])
        rs_own.start()
        rs_own.wait()
        wait_all(n, rs_copy)
        total = parts[0].astype(F32)
        for j in range(1, n):
            total = total + parts[j].astype(F32)
        mean_block[...] = total.astype(BF16)
        start_all(n, ag_copy)
        ag_own = pltpu.make_async_copy(mean_block, row_block(whole, me, piece), own_sems.at[3])
        ag_own.start()
        ag_own.wait()
        wait_all(n, ag_copy)
        gwk_out[...] = whole[:, :kv_width].astype(F32)
        gwv_out[...] = whole[:, kv_width:].astype(F32)
    wait_all(n, q_copy)


def split_bits(gate):
    first = lax.reduce_precision(gate, 8, 7)
    second = lax.reduce_precision(gate - first, 8, 7)
    third = lax.reduce_precision(gate - first - second, 8, 7)
    return first, second, third


def per_device(n, m, inputs, w_key, w_value, queries, cotangent, cum_gate):
    seq_count, positions, feature_count = inputs.shape
    rows, kv_width = w_key.shape
    kv_heads = kv_width // HD
    query_width = queries.shape[2]
    width = query_width // n
    heads = width // HD
    length = positions * n
    dma = pltpu.SemaphoreType.DMA

    def params(cid):
        return pltpu.CompilerParams(
            collective_id=cid, has_side_effects=True, vmem_limit_bytes=60 * 1024 * 1024
        )

    def shape(dims, dtype=BF16):
        return jax.ShapeDtypeStruct(dims, dtype)

    def blocks(x):
        if width % LANES == 0:
            return x.reshape(positions, query_width)
        return x.reshape(positions, n, width).transpose(1, 0, 2)

    first, second, third = split_bits(cum_gate[0])
    one = jnp.ones_like(first)
    zero = jnp.zeros_like(first)
    pad = [zero] * (HD - 6)
    gate_q = jnp.stack([one, one, one, first, second, third] + pad, axis=2).astype(BF16)
    gate_k = jnp.stack([-first, -second, -third, one, one, one] + pad, axis=2).astype(BF16)

    q_all, g_all, kv_all, w_all, x_all = pl.pallas_call(
        functools.partial(gather_kernel, n, m, width, kv_heads),
        out_shape=(
            shape((length, width)),
            shape((length, width)),
            shape((length, 2 * HD)),
            shape((rows * m, 2 * kv_width)),
            shape((m, positions, rows)),
        ),
        in_specs=[VMEM] * 5,
        out_specs=(VMEM,) * 5,
        scratch_shapes=[
            pltpu.VMEM((positions, 2 * kv_width), BF16),
            dma((2, n)), dma((2, n)), dma((2, n)),
            dma((2, m)), dma((2, m)), dma((2, m)), dma((6,)),
        ],
        compiler_params=params(0),
        name="gather_heads",
    )(blocks(queries), blocks(cotangent), inputs[0], w_key, w_value)

    tile = 256
    dq, dkv, grad_cum = pl.pallas_call(
        functools.partial(attend_kernel, heads, tile),
        out_shape=(
            shape((length, width)),
            shape((length, 2 * HD)),
            shape((heads, length), F32),
        ),
        in_specs=[VMEM] * 5,
        out_specs=(VMEM,) * 3,
        scratch_shapes=[
            pltpu.VMEM((heads, length, LANES), BF16),
            pltpu.VMEM((HD, length), BF16),
            pltpu.VMEM((length, HD), BF16),
            pltpu.VMEM((heads, length, LANES), BF16),
            pltpu.VMEM((heads, length, LANES), BF16),
            pltpu.VMEM((heads, length, HD), BF16),
            pltpu.VMEM((heads, length, tile), F32),
            pltpu.VMEM((heads, length, tile), F32),
            pltpu.VMEM((length, LANES), F32),
            pltpu.VMEM((length, HD), F32),
        ],
        compiler_params=pltpu.CompilerParams(vmem_limit_bytes=60 * 1024 * 1024),
        name="attend",
    )(q_all, g_all, kv_all, gate_q, gate_k)

    piece = rows // n
    reduce_here = rows % (16 * n) == 0
    gq_shape = (positions, query_width) if width % LANES == 0 else (n, positions, width)
    share_shape = (rows, 2 * kv_width)
    out_shape = [shape(gq_shape), shape((positions, feature_count))]
    scratch = [
        pltpu.VMEM((n, positions, 2 * HD), BF16),
        pltpu.VMEM((m, positions, 2 * kv_width), BF16),
    ]
    sems = [dma((2, n)), dma((2, n)), dma((2, m)), dma((4,))]
    if reduce_here:
        out_shape += [shape((rows, kv_width), F32)] * 2
        scratch += [
            pltpu.VMEM(share_shape, BF16),
            pltpu.VMEM((n, piece, 2 * kv_width), BF16),
            pltpu.VMEM((piece, 2 * kv_width), BF16),
            pltpu.VMEM(share_shape, BF16),
        ]
        sems += [dma((2, n)), dma((2, n))]
    else:
        out_shape += [shape(share_shape)]
    results = pl.pallas_call(
        functools.partial(return_kernel, n, m, width, kv_heads, reduce_here),
        out_shape=tuple(out_shape),
        in_specs=[VMEM] * 4,
        out_specs=(VMEM,) * len(out_shape),
        scratch_shapes=scratch + sems,
        compiler_params=params(1),
        name="return_tokens",
    )(dq, dkv, x_all, w_all)
    grad_queries, grad_input = results[:2]
    if width % LANES:
        grad_queries = grad_queries.transpose(1, 0, 2)
    if reduce_here:
        grad_wk, grad_wv = results[2:]
    else:
        summed = lax.psum(results[2], "sp").astype(F32)
        grad_wk, grad_wv = summed[:, :kv_width], summed[:, kv_width:]
    return (
        grad_input.reshape(inputs.shape),
        grad_queries.reshape(queries.shape),
        grad_cum.reshape(cum_gate.shape),
        grad_wk,
        grad_wv,
    )


def solution(mesh):
    in_specs = (
        P("dp", "sp", None),
        P("dp", None),
        P("dp", None),
        P("dp", "sp", None),
        P("dp", "sp", None),
        P("dp", "sp", None),
    )
    out_specs = (
        P("dp", "sp", None),
        P("dp", "sp", None),
        P("dp", "sp", None),
        P("dp", None),
        P("dp", None),
    )
    body = functools.partial(per_device, mesh.shape["sp"], mesh.shape["dp"])
    return jax.shard_map(
        body, mesh=mesh, in_specs=in_specs, out_specs=out_specs, check_vma=False
    )
```

profile of v0, /device:TPU:0, one launch (start us, length us, event | category | flops | bytes accessed | tf_op | source)
XLA Modules:
  0.0 196.2 jit_solution(11407755679055516535)
XLA Ops:
  0.6 0.0 copy-start.2
  0.6 0.8 bitcast_reduce-precision_fusion
  1.4 0.6 copy.14
  2.1 0.0 copy-done.2
  2.1 2.0 %copy.13 = f32[2,2048,1]{2,1,0:T(8,128)} copy(f32[2,2048,1]{1,0,2:T(2,128)S(1)} %bitcast.15) | data formatting | bytes 32768 | tf_op jit(solution)/shard_map/squeeze | solution.py:404
  4.1 3.4 %negate_convert_fusion = (bf16[2,2048,1]{2,1,0:T(8,128)(2,1)}, f32[2,2048,1]{2,1,0:T(8,128)S(1)}, bf16[2,2048,1]{2,1,0:T(8,128)(2,1)}) fusion(f32[2,2048,1]{2,1,0:T(8,128)} %copy.13, f32[2,2048,1]{2,1,0:T(8,128)S(1)} %copy.14), kind=kLoop, calls=%fused_computation.5 | loop fusion | flops 32768 | bytes 65536 | tf_op jit(solution)/shard_map/convert.2
  7.5 1.9 fusion.1
  9.5 0.1 broadcast.42
  9.6 0.1 broadcast.43
  9.8 0.1 broadcast.44
  9.9 1.1 broadcast.45
  11.0 1.1 broadcast.46
  12.1 1.1 broadcast.47
  13.3 9.9 %stack.7.gate_k = bf16[2,2048,64]{2,1,0:T(8,128)(2,1)} concatenate(bf16[2,2048,1]{2,1,0:T(8,128)(2,1)} %get-tuple-element.34, bf16[2,2048,1]{2,1,0:T(8,128)(2,1)} %get-tuple-element.31, bf16[2,2048,1]{2,1,0:T(8,128)(2,1)} %get-tuple-element.29, bf16[2,2048,1]{2,1,0:T(8,128)(2,1)S(1)} %broadcast.42, bf16[2,2048,2]{2,1,0:T(8,128)(2,1)S(1)} %broadcast.43, ...), dimensions={2} | concatenate | bytes 1048576 | tf_op jit(solution)/shard_map/stack | solution.py:409
  23.2 1.4 copy.15
  24.6 10.1 %stack.6.gate_q = bf16[2,2048,64]{2,1,0:T(8,128)(2,1)} concatenate(bf16[2,2048,1]{2,1,0:T(8,128)(2,1)S(1)} %broadcast.42, bf16[2,2048,2]{2,1,0:T(8,128)(2,1)S(1)} %broadcast.43, bf16[2,2048,1]{2,1,0:T(8,128)(2,1)} %copy.15, bf16[2,2048,1]{2,1,0:T(8,128)(2,1)} %get-tuple-element.33, bf16[2,2048,1]{2,1,0:T(8,128)(2,1)} %get-tuple-element.32, bf16[2,2048,2]{2,1,0:T(8,128)(2,1)S(1)} %broadcast.44, ...), dimensions={2} | concatenate | bytes 1048576 | tf_op jit(solution)/shard_map/stack | solution.py:408
  34.7 42.0 %gather_heads.1 = (bf16[2048,128]{1,0:T(8,128)(2,1)}, bf16[2048,128]{1,0:T(8,128)(2,1)}, bf16[2048,128]{1,0:T(8,128)(2,1)}, bf16[2048,512]{1,0:T(8,128)(2,1)}, bf16[2,128,1024]{2,1,0:T(8,128)(2,1)}) custom-call(bf16[128,2048]{1,0:T(8,128)(2,1)} %bitcast.10, bf16[128,2048]{1,0:T(8,128)(2,1)} %bitcast.11, bf16[128,2048]{1,0:T(8,128)(2,1)} %bitcast.12, ...), custom_call_target="tpu_custom_call" | custom-call | tf_op jit(solution)/shard_map/gather_heads/pallas_call | solution.py:411
  76.8 35.3 %attend.1 = (bf16[2048,128]{1,0:T(8,128)(2,1)}, bf16[2048,128]{1,0:T(8,128)(2,1)}, f32[2,2048]{1,0:T(2,128)}) custom-call(bf16[2048,128]{1,0:T(8,128)(2,1)} %get-tuple-element.17.q_ref, bf16[2048,128]{1,0:T(8,128)(2,1)} %get-tuple-element.18.g_ref, bf16[2048,128]{1,0:T(8,128)(2,1)} %get-tuple-element.19.kv_ref, bf16[2,2048,64]{2,1,0:T(8,128)(2,1)} %stack.6.gate_q, ...), custom_call_target="tpu_custom_call" | custom-call | tf_op jit(solution)/shard_map/attend/pallas_call | solution.py:432
  112.1 78.3 %return_tokens.1 = (bf16[128,2048]{1,0:T(8,128)(2,1)}, bf16[128,2048]{1,0:T(8,128)(2,1)}, f32[1024,256]{1,0:T(8,128)}, f32[1024,256]{1,0:T(8,128)}) custom-call(bf16[2048,128]{1,0:T(8,128)(2,1)} %get-tuple-element.20.dq_ref, bf16[2048,128]{1,0:T(8,128)(2,1)} %get-tuple-element.21.dkv_ref, bf16[2,128,1024]{2,1,0:T(8,128)(2,1)} %get-tuple-element.22.x_ref, ...), custom_call_target="tpu_custom_call" | custom-call | tf_op jit(solution)/shard_map/return_tokens/pallas_call | solution.py:478
  190.4 0.0 copy-start.1
  190.4 0.0 copy-start
  190.4 2.0 %copy.21 = bf16[1,128,2048]{2,1,0:T(8,128)(2,1)} copy(bf16[1,128,2048]{2,1,0:T(8,128)(2,1)} %bitcast.14) | data formatting | bytes 1048576
  192.4 1.9 copy.22
  194.3 0.0 copy-done.1
  194.3 1.0 copy.23
  195.3 0.0 copy-done
  195.3 1.0 copy.24
Async XLA Ops:
  0.6 1.5 copy-start.2
  190.4 3.9 %copy-start.1 = (f32[1024,256]{1,0:T(8,128)S(1)}, f32[1024,256]{1,0:T(8,128)}, u32[]{:S(2)}) copy-start(f32[1024,256]{1,0:T(8,128)} %get-tuple-element.45) | copy-start | bytes 3145732
  190.4 4.9 %copy-start = (f32[1024,256]{1,0:T(8,128)S(1)}, f32[1024,256]{1,0:T(8,128)}, u32[]{:S(2)}) copy-start(f32[1024,256]{1,0:T(8,128)} %get-tuple-element.46) | copy-start | bytes 3145732
where the time goes:
time: 200 us; the launch traced here: 196 us
  Pallas kernels  156 us (78%)
  local copies, waits for them, and re-layouts  33.7 us (17%)
  other arithmetic  6.18 us (3%)
    pallas_call x1, Pallas kernels, per_device(): pl.pallas_call(functools.partial(return_kernel, n, m, width, kv_heads, re...  78.3 us
    pallas_call x1, Pallas kernels, per_device(): pl.pallas_call(functools.partial(gather_kernel, n, m, width, kv_heads), o...  42 us
    pallas_call x1, Pallas kernels, per_device(): pl.pallas_call(functools.partial(attend_kernel, heads, tile), out_shape=(...  35.3 us
    another operation x1, local copies, waits for them, and re-layouts, per_device(): jnp.stack([one, one, one, first, second, third] + pad, axis=2).astype(BF16)  10.1 us
    another operation x1, local copies, waits for them, and re-layouts, per_device(): jnp.stack([-first, -second, -third, one, one, one] + pad, axis=2)  9.95 us
    unnamed x10, local copies, waits for them, and re-layouts  5.86 us
    another operation x2, other arithmetic  5.39 us
    another operation x7, local copies, waits for them, and re-layouts  5.17 us

commit v1 on v0

--- a/solution.py
+++ b/solution.py
@@ -84,9 +84,11 @@
     n, m, width, kv_heads,
     q_ref, g_ref, x_ref, wk_ref, wv_ref,
     q_out, g_out, kv_out, w_out, x_out,
-    kv_block, q_sems, g_sems, kv_sems, wk_sems, wv_sems, x_sems, own_sems,
+    kv_block, q_sems, g_sems, kv_sems, mate_sems, wk_sems, wv_sems, x_sems, own_sems,
 ):
     me, mine = lax.axis_index("sp"), lax.axis_index("dp")
+    per = n // kv_heads
+    plane, member = me // per, lax.rem(me, per)
     positions = x_ref.shape[0]
     rows, kv_width = wk_ref.shape
     greet(n, m)
@@ -123,10 +125,18 @@
         )
 
     def kv_copy(k):
-        group = (target(k) * kv_heads) // n
+        group = lax.rem(plane + k, kv_heads)
         return remote(
             column_block(kv_block, group, 2 * HD),
-            row_block(kv_out, me, positions), kv_sems, k, {"sp": target(k)},
+            row_block(kv_out, me, positions), kv_sems, k, {"sp": group * per + member},
+        )
+
+    def mate_copy(k, step):
+        source = lax.rem(plane - step + kv_heads, kv_heads) * per + member
+        rows_of = row_block(kv_out, source, positions)
+        return remote(
+            rows_of, rows_of, mate_sems.at[step], k,
+            {"sp": plane * per + lax.rem(member + k, per)},
         )
 
     own = [
@@ -147,12 +157,10 @@
     start_all(m, wk_copy)
     start_all(m, wv_copy)
     start_all(n, q_copy)
-    start_all(n, g_copy)
     for copy in own:
         copy.start()
     wait_all(m, wk_copy)
     wait_all(m, wv_copy)
-    start_all(m, x_copy)
     for copy in own:
         copy.wait()
     both = dot_nn(x_ref[...], w_out[...]).astype(BF16)
@@ -161,37 +169,121 @@
         pieces.append(both[:, group * HD : (group + 1) * HD])
         pieces.append(both[:, kv_width + group * HD : kv_width + (group + 1) * HD])
     kv_block[...] = jnp.concatenate(pieces, axis=1)
-    start_all(n, kv_copy)
+    start_all(kv_heads, kv_copy)
     kv_own = pltpu.make_async_copy(
-        column_block(kv_block, (me * kv_heads) // n, 2 * HD),
+        column_block(kv_block, plane, 2 * HD),
         row_block(kv_out, me, positions), own_sems.at[5],
     )
     kv_own.start()
+    start_all(n, g_copy)
+    start_all(m, x_copy)
     kv_own.wait()
+    start_all(per, lambda k: mate_copy(k, 0))
+
+    @pl.loop(1, kv_heads)
+    def _(step):
+        kv_copy(step).wait()
+        start_all(per, lambda k: mate_copy(k, step))
+
     wait_all(m, x_copy)
     wait_all(n, q_copy)
     wait_all(n, g_copy)
-    wait_all(n, kv_copy)
+
+    @pl.loop(0, kv_heads)
+    def _(step):
+        wait_all(per, lambda k: mate_copy(k, step))
+
+
+def split_bits(gate):
+    first = gate.astype(BF16).astype(F32)
+    second = (gate - first).astype(BF16).astype(F32)
+    third = (gate - first - second).astype(BF16).astype(F32)
+    return first, second, third
 
 
 def attend_kernel(
-    heads, tile,
-    q_ref, g_ref, kv_ref, gate_q, gate_k,
-    dq_ref, dkv_ref, gc_ref,
-    kx, kt, vs, qx, qd, gh, s_buf, d_buf, dk_acc, dv_acc,
+    n, m, width, kv_heads, tile, reduce_here,
+    q_ref, g_ref, kv_ref, gate_ref, x_ref, w_ref,
+    gq_out, gx_out, gc_ref, *rest,
 ):
+    if reduce_here:
+        (gwk_out, gwv_out, *rest, share, parts, mean_block, whole, rs_sems, ag_sems) = rest
+    else:
+        share, *rest = rest
+    (kx, kt, vs, qx, qd, gh, s_buf, d_buf, dk_acc, dv_acc, dq_buf, dkv_buf,
+     slots, sums_buf, groups_buf, gkv_all,
+     q_sems, mate_sems, group_sems, gkv_sems, own_sems) = rest
+    me, mine = lax.axis_index("sp"), lax.axis_index("dp")
+    heads = width // HD
     length = kv_ref.shape[0]
+    positions = gx_out.shape[0]
+    kv_width = kv_heads * HD
+    per = n // kv_heads
+    plane, member = me // per, lax.rem(me, per)
     scale = HD ** (-0.5)
+    greet(n, m)
+
+    def target(k):
+        return lax.rem(me + k, n)
+
+    def peer(k):
+        return lax.rem(mine + k, m)
+
+    def q_copy(k):
+        return remote(
+            row_block(dq_buf, target(k), positions),
+            column_block(gq_out, me, width), q_sems, k, {"sp": target(k)},
+        )
+
+    def mate_copy(k, a):
+        to = lax.rem(member + k, per)
+        return remote(
+            row_block(dkv_buf, a * per + to, positions), slots.at[member, a],
+            mate_sems.at[a], k, {"sp": plane * per + to},
+        )
+
+    def group_copy(k):
+        a = lax.rem(plane + k, kv_heads)
+        return remote(
+            sums_buf.at[a], groups_buf.at[plane], group_sems, k, {"sp": a * per + member}
+        )
+
+    def gkv_copy(k):
+        return remote(gkv_all.at[mine], gkv_all.at[mine], gkv_sems, k, {"dp": peer(k)})
+
+    q_own = pltpu.make_async_copy(
+        row_block(dq_buf, me, positions), column_block(gq_out, me, width), own_sems.at[0]
+    )
+
+    def send_tile(i):
+        for part in range(tile // positions):
+            j = i * (tile // positions) + part
+            k = lax.rem(j - me + n, n)
+            a, b = j // per, lax.rem(j, per)
+            km = lax.rem(b - member + per, per)
+
+            @pl.when(km != 0)
+            def _():
+                mate_copy(km, a).start()
+
+            @pl.when(k != 0)
+            def _():
+                q_copy(k).start()
+
     keys = kv_ref[:, :HD]
     kt[...] = keys.astype(F32).T.astype(BF16)
     vs[...] = kv_ref[:, HD:]
     dk_acc[...] = jnp.zeros_like(dk_acc)
     dv_acc[...] = jnp.zeros_like(dv_acc)
     lane = lax.broadcasted_iota(jnp.int32, (length, HD), 1)
+    ones = jnp.ones((3, length), F32)
+    blank = jnp.zeros((HD - 6, length), F32)
     for h in range(heads):
+        three = jnp.concatenate(split_bits(gate_ref[h : h + 1, :]), axis=0)
+        gates = jnp.concatenate([ones, three, blank, -three, ones, blank], axis=0).T.astype(BF16)
         q_head = q_ref[:, h * HD : (h + 1) * HD]
-        kx[h] = jnp.concatenate([keys, gate_k[h]], axis=1)
-        qx[h] = jnp.concatenate([q_head * jnp.asarray(scale, BF16), gate_q[h]], axis=1)
+        kx[h] = jnp.concatenate([keys, gates[:, HD:]], axis=1)
+        qx[h] = jnp.concatenate([q_head * jnp.asarray(scale, BF16), gates[:, :HD]], axis=1)
         mark = jnp.where(lane == h, 1.0, 0.0).astype(BF16)
         qd[h] = jnp.concatenate([q_head, mark], axis=1)
         gh[h] = g_ref[:, h * HD : (h + 1) * HD]
@@ -203,8 +295,11 @@
     def fold(op, a):
         return op(a.reshape(tile // 8, 8, tile), axis=0)
 
-    @pl.loop(0, length // tile)
-    def _(i):
+    tiles = length // tile
+
+    @pl.loop(0, tiles)
+    def _(turn):
+        i = tiles - 1 - turn
         here = pl.ds(pl.multiple_of(i * tile, tile), tile)
 
         def score(c, tops, diagonal):
@@ -263,73 +358,40 @@
 
         start = tuple(jnp.zeros((HD, tile), F32) for _ in every)
         grads = lax.fori_loop(0, i + 1, spread, start)
-        dq_ref[here, :] = jnp.concatenate([(gr.T * scale) for gr in grads], axis=1).astype(BF16)
-
-    dk = dk_acc[...]
-    dkv_ref[...] = jnp.concatenate([dk[:, :HD] * scale, dv_acc[...]], axis=1).astype(BF16)
-    columns = dk.T
+        dq_buf[here, :] = jnp.concatenate([gr.T * scale for gr in grads], axis=1).astype(BF16)
+        dkv_buf[here, :] = jnp.concatenate(
+            [dk_acc[here, :][:, :HD] * scale, dv_acc[here, :]], axis=1
+        ).astype(BF16)
+
+        @pl.when(turn > 0)
+        def _():
+            send_tile(i + 1)
+
+    send_tile(0)
+    q_own.start()
+    columns = dk_acc[...].T
     gc_ref[...] = gc_ref[...] - columns[HD : HD + heads, :]
 
-
-def return_kernel(
-    n, m, width, kv_heads, reduce_here,
-    dq_ref, dkv_ref, x_ref, w_ref,
-    gq_out, gx_out, *rest,
-):
-    if reduce_here:
-        (gwk_out, gwv_out, slots, gkv_all, share, parts, mean_block, whole,
-         q_sems, kv_sems, gkv_sems, own_sems, rs_sems, ag_sems) = rest
-    else:
-        share, slots, gkv_all, q_sems, kv_sems, gkv_sems, own_sems = rest
-    me, mine = lax.axis_index("sp"), lax.axis_index("dp")
-    positions = slots.shape[1]
-    kv_width = kv_heads * HD
-    greet(n, m)
-
-    def target(k):
-        return lax.rem(me + k, n)
-
-    def peer(k):
-        return lax.rem(mine + k, m)
-
-    def q_copy(k):
-        return remote(
-            row_block(dq_ref, target(k), positions),
-            column_block(gq_out, me, width), q_sems, k, {"sp": target(k)},
-        )
-
-    def kv_copy(k):
-        return remote(
-            row_block(dkv_ref, target(k), positions), slots.at[me], kv_sems, k,
-            {"sp": target(k)},
-        )
-
-    def gkv_copy(k):
-        return remote(gkv_all.at[mine], gkv_all.at[mine], gkv_sems, k, {"dp": peer(k)})
-
-    start_all(n, kv_copy)
-    start_all(n, q_copy)
-    kv_own = pltpu.make_async_copy(
-        row_block(dkv_ref, me, positions), slots.at[me], own_sems.at[0]
-    )
-    q_own = pltpu.make_async_copy(
-        row_block(dq_ref, me, positions), column_block(gq_out, me, width), own_sems.at[1]
-    )
-    kv_own.start()
-    q_own.start()
-    kv_own.wait()
-    q_own.wait()
-    wait_all(n, kv_copy)
-    per = n // kv_heads
-    groups = []
-    for group in range(kv_heads):
-        total = slots[group * per].astype(F32)
-        for j in range(1, per):
-            total = total + slots[group * per + j].astype(F32)
-        groups.append(total)
+    @pl.loop(0, kv_heads)
+    def _(step):
+        a = lax.rem(plane + 1 + step, kv_heads)
+        wait_all(per, lambda k: mate_copy(k, a))
+        rows_of = row_block(dkv_buf, a * per + member, positions)
+        total = rows_of[...].astype(F32)
+        for k in range(1, per):
+            total = total + slots[lax.rem(member + k, per), a].astype(F32)
+        sums_buf[a] = total.astype(BF16)
+
+        @pl.when(step < kv_heads - 1)
+        def _():
+            group_copy(step + 1).start()
+
+    groups_buf[plane] = sums_buf[plane]
+    wait_all(kv_heads, group_copy)
+    groups = [groups_buf[group] for group in range(kv_heads)]
     gkv = jnp.concatenate(
         [total[:, :HD] for total in groups] + [total[:, HD:] for total in groups], axis=1
-    ).astype(BF16)
+    )
     gkv_all[mine] = gkv
     start_all(m, gkv_copy)
     gx_out[...] = dot_nt(gkv, w_ref[...]).astype(BF16)
@@ -353,7 +415,7 @@
             )
 
         start_all(n, rs_copy)
-        rs_own = pltpu.make_async_copy(row_block(share, me, piece), parts.at[me], own_sems.at[2])
+        rs_own = pltpu.make_async_copy(row_block(share, me, piece), parts.at[me], own_sems.at[1])
         rs_own.start()
         rs_own.wait()
         wait_all(n, rs_copy)
@@ -362,20 +424,14 @@
             total = total + parts[j].astype(F32)
         mean_block[...] = total.astype(BF16)
         start_all(n, ag_copy)
-        ag_own = pltpu.make_async_copy(mean_block, row_block(whole, me, piece), own_sems.at[3])
+        ag_own = pltpu.make_async_copy(mean_block, row_block(whole, me, piece), own_sems.at[2])
         ag_own.start()
         ag_own.wait()
         wait_all(n, ag_copy)
         gwk_out[...] = whole[:, :kv_width].astype(F32)
         gwv_out[...] = whole[:, kv_width:].astype(F32)
+    q_own.wait()
     wait_all(n, q_copy)
-
-
-def split_bits(gate):
-    first = lax.reduce_precision(gate, 8, 7)
-    second = lax.reduce_precision(gate - first, 8, 7)
-    third = lax.reduce_precision(gate - first - second, 8, 7)
-    return first, second, third
 
 
 def per_device(n, m, inputs, w_key, w_value, queries, cotangent, cum_gate):
@@ -400,13 +456,6 @@
         if width % LANES == 0:
             return x.reshape(positions, query_width)
         return x.reshape(positions, n, width).transpose(1, 0, 2)
-
-    first, second, third = split_bits(cum_gate[0])
-    one = jnp.ones_like(first)
-    zero = jnp.zeros_like(first)
-    pad = [zero] * (HD - 6)
-    gate_q = jnp.stack([one, one, one, first, second, third] + pad, axis=2).astype(BF16)
-    gate_k = jnp.stack([-first, -second, -third, one, one, one] + pad, axis=2).astype(BF16)
 
     q_all, g_all, kv_all, w_all, x_all = pl.pallas_call(
         functools.partial(gather_kernel, n, m, width, kv_heads),
@@ -421,49 +470,41 @@
         out_specs=(VMEM,) * 5,
         scratch_shapes=[
             pltpu.VMEM((positions, 2 * kv_width), BF16),
-            dma((2, n)), dma((2, n)), dma((2, n)),
+            dma((2, n)), dma((2, n)), dma((2, kv_heads)), dma((kv_heads, 2, n // kv_heads)),
             dma((2, m)), dma((2, m)), dma((2, m)), dma((6,)),
         ],
         compiler_params=params(0),
         name="gather_heads",
     )(blocks(queries), blocks(cotangent), inputs[0], w_key, w_value)
 
-    tile = 256
-    dq, dkv, grad_cum = pl.pallas_call(
-        functools.partial(attend_kernel, heads, tile),
-        out_shape=(
-            shape((length, width)),
-            shape((length, 2 * HD)),
-            shape((heads, length), F32),
-        ),
-        in_specs=[VMEM] * 5,
-        out_specs=(VMEM,) * 3,
-        scratch_shapes=[
-            pltpu.VMEM((heads, length, LANES), BF16),
-            pltpu.VMEM((HD, length), BF16),
-            pltpu.VMEM((length, HD), BF16),
-            pltpu.VMEM((heads, length, LANES), BF16),
-            pltpu.VMEM((heads, length, LANES), BF16),
-            pltpu.VMEM((heads, length, HD), BF16),
-            pltpu.VMEM((heads, length, tile), F32),
-            pltpu.VMEM((heads, length, tile), F32),
-            pltpu.VMEM((length, LANES), F32),
-            pltpu.VMEM((length, HD), F32),
-        ],
-        compiler_params=pltpu.CompilerParams(vmem_limit_bytes=60 * 1024 * 1024),
-        name="attend",
-    )(q_all, g_all, kv_all, gate_q, gate_k)
-
+    tile = max(256, positions)
     piece = rows // n
     reduce_here = rows % (16 * n) == 0
     gq_shape = (positions, query_width) if width % LANES == 0 else (n, positions, width)
     share_shape = (rows, 2 * kv_width)
-    out_shape = [shape(gq_shape), shape((positions, feature_count))]
+    per = n // kv_heads
+    out_shape = [
+        shape(gq_shape), shape((positions, feature_count)), shape((heads, length), F32)
+    ]
     scratch = [
-        pltpu.VMEM((n, positions, 2 * HD), BF16),
+        pltpu.VMEM((heads, length, LANES), BF16),
+        pltpu.VMEM((HD, length), BF16),
+        pltpu.VMEM((length, HD), BF16),
+        pltpu.VMEM((heads, length, LANES), BF16),
+        pltpu.VMEM((heads, length, LANES), BF16),
+        pltpu.VMEM((heads, length, HD), BF16),
+        pltpu.VMEM((heads, length, tile), F32),
+        pltpu.VMEM((heads, length, tile), F32),
+        pltpu.VMEM((length, LANES), F32),
+        pltpu.VMEM((length, HD), F32),
+        pltpu.VMEM((length, width), BF16),
+        pltpu.VMEM((length, 2 * HD), BF16),
+        pltpu.VMEM((per, kv_heads, positions, 2 * HD), BF16),
+        pltpu.VMEM((kv_heads, positions, 2 * HD), BF16),
+        pltpu.VMEM((kv_heads, positions, 2 * HD), BF16),
         pltpu.VMEM((m, positions, 2 * kv_width), BF16),
+        dma((2, n)), dma((kv_heads, 2, per)), dma((2, kv_heads)), dma((2, m)), dma((3,)),
     ]
-    sems = [dma((2, n)), dma((2, n)), dma((2, m)), dma((4,))]
     if reduce_here:
         out_shape += [shape((rows, kv_width), F32)] * 2
         scratch += [
@@ -471,26 +512,26 @@
             pltpu.VMEM((n, piece, 2 * kv_width), BF16),
             pltpu.VMEM((piece, 2 * kv_width), BF16),
             pltpu.VMEM(share_shape, BF16),
+            dma((2, n)), dma((2, n)),
         ]
-        sems += [dma((2, n)), dma((2, n))]
     else:
         out_shape += [shape(share_shape)]
     results = pl.pallas_call(
-        functools.partial(return_kernel, n, m, width, kv_heads, reduce_here),
+        functools.partial(attend_kernel, n, m, width, kv_heads, tile, reduce_here),
         out_shape=tuple(out_shape),
-        in_specs=[VMEM] * 4,
+        in_specs=[VMEM] * 6,
         out_specs=(VMEM,) * len(out_shape),
-        scratch_shapes=scratch + sems,
+        scratch_shapes=scratch,
         compiler_params=params(1),
-        name="return_tokens",
-    )(dq, dkv, x_all, w_all)
-    grad_queries, grad_input = results[:2]
+        name="attend_return",
+    )(q_all, g_all, kv_all, cum_gate[0], x_all, w_all)
+    grad_queries, grad_input, grad_cum = results[:3]
     if width % LANES:
         grad_queries = grad_queries.transpose(1, 0, 2)
     if reduce_here:
-        grad_wk, grad_wv = results[2:]
+        grad_wk, grad_wv = results[3:]
     else:
-        summed = lax.psum(results[2], "sp").astype(F32)
+        summed = lax.psum(results[3], "sp").astype(F32)
         grad_wk, grad_wv = summed[:, :kv_width], summed[:, kv_width:]
     return (
         grad_input.reshape(inputs.shape),

time: 200 us -> 156 us (0.78)
  the two profiles are of different devices: /device:TPU:0 before, /device:TPU:30 now
where the time goes in v1:
time: 156 us
  Pallas kernels  149 us (96%)
  local copies, waits for them, and re-layouts  6.47 us (4%)
    pallas_call x1, Pallas kernels, per_device(): pl.pallas_call(functools.partial(attend_kernel, n, m, width, kv_heads, ti...  114 us
    pallas_call x1, Pallas kernels, per_device(): pl.pallas_call(functools.partial(gather_kernel, n, m, width, kv_heads), o...  35.3 us
    unnamed x11, local copies, waits for them, and re-layouts  6.47 us

profile of v1, /device:TPU:30, one launch (start us, length us, event | category | flops | bytes accessed | tf_op | source)
XLA Modules:
  0.0 156.2 jit_solution(4506388091553638899)
XLA Ops:
  0.6 35.3 %gather_heads.1 = (bf16[2048,128]{1,0:T(8,128)(2,1)}, bf16[2048,128]{1,0:T(8,128)(2,1)}, bf16[2048,128]{1,0:T(8,128)(2,1)}, bf16[2048,512]{1,0:T(8,128)(2,1)}, bf16[2,128,1024]{2,1,0:T(8,128)(2,1)}) custom-call(bf16[128,2048]{1,0:T(8,128)(2,1)} %bitcast.7, bf16[128,2048]{1,0:T(8,128)(2,1)} %bitcast.8, bf16[128,2048]{1,0:T(8,128)(2,1)} %bitcast.9, ...), custom_call_target="tpu_custom_call" | custom-call | tf_op jit(solution)/shard_map/gather_heads/pallas_call | solution.py:460
  35.9 113.8 %attend_return.1 = (bf16[128,2048]{1,0:T(8,128)(2,1)}, bf16[128,2048]{1,0:T(8,128)(2,1)}, f32[2,2048]{1,0:T(2,128)}, f32[1024,256]{1,0:T(8,128)}, f32[1024,256]{1,0:T(8,128)}) custom-call(bf16[2048,128]{1,0:T(8,128)(2,1)} %get-tuple-element.15.q_ref, bf16[2048,128]{1,0:T(8,128)(2,1)} %get-tuple-element.16.g_ref, bf16[2048,128]{1,0:T(8,128)(2,1)} %get-tuple-element.17.kv_ref, ...), custom_call_target="tpu_custom_call" | custom-call | tf_op jit(solution)/shard_map/attend_return/pallas_call | solution.py:519
  149.7 0.0 copy-start.2
  149.7 0.0 copy-start.1
  149.7 0.0 copy-start
  149.7 2.0 %copy.16 = bf16[1,128,2048]{2,1,0:T(8,128)(2,1)} copy(bf16[1,128,2048]{2,1,0:T(8,128)(2,1)} %bitcast.11) | data formatting | bytes 1048576
  151.7 1.9 %copy.17 = bf16[1,128,2048]{2,1,0:T(8,128)(2,1)} copy(bf16[1,128,2048]{2,1,0:T(8,128)(2,1)} %bitcast.10) | data formatting | bytes 1048576
  153.6 0.0 copy-done.2
  153.6 0.6 copy.18
  154.2 0.0 copy-done.1
  154.2 1.0 copy.19
  155.2 0.0 copy-done
  155.2 1.0 copy.20
Async XLA Ops:
  149.7 3.9 %copy-start.2 = (f32[2,2048]{1,0:T(2,128)S(1)}, f32[2,2048]{1,0:T(2,128)}, u32[]{:S(2)}) copy-start(f32[2,2048]{1,0:T(2,128)} %get-tuple-element.22) | copy-start | bytes 49156
  149.7 4.5 %copy-start.1 = (f32[1024,256]{1,0:T(8,128)S(1)}, f32[1024,256]{1,0:T(8,128)}, u32[]{:S(2)}) copy-start(f32[1024,256]{1,0:T(8,128)} %get-tuple-element.33) | copy-start | bytes 3145732
  149.7 5.5 %copy-start = (f32[1024,256]{1,0:T(8,128)S(1)}, f32[1024,256]{1,0:T(8,128)}, u32[]{:S(2)}) copy-start(f32[1024,256]{1,0:T(8,128)} %get-tuple-element.34) | copy-start | bytes 3145732

commit v2 on v1

--- a/solution.py
+++ b/solution.py
@@ -80,17 +80,36 @@
     return ref.at[pl.ds(pl.multiple_of(j * rows, 16), rows)]
 
 
-def gather_kernel(
-    n, m, width, kv_heads,
-    q_ref, g_ref, x_ref, wk_ref, wv_ref,
-    q_out, g_out, kv_out, w_out, x_out,
-    kv_block, q_sems, g_sems, kv_sems, mate_sems, wk_sems, wv_sems, x_sems, own_sems,
+def split_bits(gate):
+    first = gate.astype(BF16).astype(F32)
+    second = (gate - first).astype(BF16).astype(F32)
+    third = (gate - first - second).astype(BF16).astype(F32)
+    return first, second, third
+
+
+def attend_kernel(
+    n, m, width, kv_heads, tile, reduce_here,
+    q_ref, g_ref, gate_ref, x_ref, wk_ref, wv_ref,
+    gq_out, gx_out, gc_ref, *rest,
 ):
+    if reduce_here:
+        (gw_out, *rest, share, parts, rs_sum, rs_groups, whole,
+         rs_mate_sems, rs_sems, ag_sems, ag_mate_sems) = rest
+    else:
+        share, *rest = rest
+    (q_all, g_all, kv_all, w_all, x_all, kv_block,
+     qi_sems, g_sems, kvi_sems, matei_sems, wk_sems, wv_sems, x_sems, owni_sems,
+     kx, kt, vs, qx, qd, gh, s_buf, d_buf, dk_acc, dv_acc, dq_buf, dkv_buf,
+     slots, sums_buf, groups_buf, gkv_all,
+     q_sems, mate_sems, group_sems, gkv_sems, own_sems) = rest
     me, mine = lax.axis_index("sp"), lax.axis_index("dp")
+    heads = width // HD
+    length = kv_all.shape[0]
+    positions = x_ref.shape[0]
+    rows, kv_width = wk_ref.shape
     per = n // kv_heads
     plane, member = me // per, lax.rem(me, per)
-    positions = x_ref.shape[0]
-    rows, kv_width = wk_ref.shape
+    scale = HD ** (-0.5)
     greet(n, m)
 
     def target(k):
@@ -100,134 +119,90 @@
         return lax.rem(mine + k, m)
 
     def wk_copy(k):
-        dst = row_block(w_out, mine, rows).at[:, pl.ds(0, kv_width)]
+        dst = row_block(w_all, mine, rows).at[:, pl.ds(0, kv_width)]
         return remote(wk_ref, dst, wk_sems, k, {"dp": peer(k)})
 
     def wv_copy(k):
-        dst = row_block(w_out, mine, rows).at[:, pl.ds(kv_width, kv_width)]
+        dst = row_block(w_all, mine, rows).at[:, pl.ds(kv_width, kv_width)]
         return remote(wv_ref, dst, wv_sems, k, {"dp": peer(k)})
 
     def x_copy(k):
         return remote(
-            column_block(x_ref, peer(k), rows), x_out.at[mine], x_sems, k, {"dp": peer(k)}
-        )
-
-    def q_copy(k):
+            column_block(x_ref, peer(k), rows), x_all.at[mine], x_sems, k, {"dp": peer(k)}
+        )
+
+    def qi_copy(k):
         return remote(
             column_block(q_ref, target(k), width),
-            row_block(q_out, me, positions), q_sems, k, {"sp": target(k)},
+            row_block(q_all, me, positions), qi_sems, k, {"sp": target(k)},
         )
 
     def g_copy(k):
         return remote(
             column_block(g_ref, target(k), width),
-            row_block(g_out, me, positions), g_sems, k, {"sp": target(k)},
-        )
-
-    def kv_copy(k):
+            row_block(g_all, me, positions), g_sems, k, {"sp": target(k)},
+        )
+
+    def kvi_copy(k):
         group = lax.rem(plane + k, kv_heads)
         return remote(
             column_block(kv_block, group, 2 * HD),
-            row_block(kv_out, me, positions), kv_sems, k, {"sp": group * per + member},
-        )
-
-    def mate_copy(k, step):
+            row_block(kv_all, me, positions), kvi_sems, k, {"sp": group * per + member},
+        )
+
+    def matei_copy(k, step):
         source = lax.rem(plane - step + kv_heads, kv_heads) * per + member
-        rows_of = row_block(kv_out, source, positions)
-        return remote(
-            rows_of, rows_of, mate_sems.at[step], k,
+        rows_of = row_block(kv_all, source, positions)
+        return remote(
+            rows_of, rows_of, matei_sems.at[step], k,
             {"sp": plane * per + lax.rem(member + k, per)},
         )
 
     own = [
         pltpu.make_async_copy(
-            wk_ref, row_block(w_out, mine, rows).at[:, pl.ds(0, kv_width)], own_sems.at[0]
+            wk_ref, row_block(w_all, mine, rows).at[:, pl.ds(0, kv_width)], owni_sems.at[0]
         ),
         pltpu.make_async_copy(
-            wv_ref, row_block(w_out, mine, rows).at[:, pl.ds(kv_width, kv_width)], own_sems.at[1]
+            wv_ref, row_block(w_all, mine, rows).at[:, pl.ds(kv_width, kv_width)], owni_sems.at[1]
         ),
-        pltpu.make_async_copy(column_block(x_ref, mine, rows), x_out.at[mine], own_sems.at[2]),
+        pltpu.make_async_copy(column_block(x_ref, mine, rows), x_all.at[mine], owni_sems.at[2]),
         pltpu.make_async_copy(
-            column_block(q_ref, me, width), row_block(q_out, me, positions), own_sems.at[3]
+            column_block(q_ref, me, width), row_block(q_all, me, positions), owni_sems.at[3]
         ),
         pltpu.make_async_copy(
-            column_block(g_ref, me, width), row_block(g_out, me, positions), own_sems.at[4]
+            column_block(g_ref, me, width), row_block(g_all, me, positions), owni_sems.at[4]
         ),
     ]
     start_all(m, wk_copy)
     start_all(m, wv_copy)
-    start_all(n, q_copy)
+    start_all(n, qi_copy)
     for copy in own:
         copy.start()
     wait_all(m, wk_copy)
     wait_all(m, wv_copy)
     for copy in own:
         copy.wait()
-    both = dot_nn(x_ref[...], w_out[...]).astype(BF16)
+    both = dot_nn(x_ref[...], w_all[...]).astype(BF16)
     pieces = []
     for group in range(kv_heads):
         pieces.append(both[:, group * HD : (group + 1) * HD])
         pieces.append(both[:, kv_width + group * HD : kv_width + (group + 1) * HD])
     kv_block[...] = jnp.concatenate(pieces, axis=1)
-    start_all(kv_heads, kv_copy)
+    start_all(kv_heads, kvi_copy)
     kv_own = pltpu.make_async_copy(
         column_block(kv_block, plane, 2 * HD),
-        row_block(kv_out, me, positions), own_sems.at[5],
+        row_block(kv_all, me, positions), owni_sems.at[5],
     )
     kv_own.start()
     start_all(n, g_copy)
     start_all(m, x_copy)
     kv_own.wait()
-    start_all(per, lambda k: mate_copy(k, 0))
+    start_all(per, lambda k: matei_copy(k, 0))
 
     @pl.loop(1, kv_heads)
     def _(step):
-        kv_copy(step).wait()
-        start_all(per, lambda k: mate_copy(k, step))
-
-    wait_all(m, x_copy)
-    wait_all(n, q_copy)
-    wait_all(n, g_copy)
-
-    @pl.loop(0, kv_heads)
-    def _(step):
-        wait_all(per, lambda k: mate_copy(k, step))
-
-
-def split_bits(gate):
-    first = gate.astype(BF16).astype(F32)
-    second = (gate - first).astype(BF16).astype(F32)
-    third = (gate - first - second).astype(BF16).astype(F32)
-    return first, second, third
-
-
-def attend_kernel(
-    n, m, width, kv_heads, tile, reduce_here,
-    q_ref, g_ref, kv_ref, gate_ref, x_ref, w_ref,
-    gq_out, gx_out, gc_ref, *rest,
-):
-    if reduce_here:
-        (gwk_out, gwv_out, *rest, share, parts, mean_block, whole, rs_sems, ag_sems) = rest
-    else:
-        share, *rest = rest
-    (kx, kt, vs, qx, qd, gh, s_buf, d_buf, dk_acc, dv_acc, dq_buf, dkv_buf,
-     slots, sums_buf, groups_buf, gkv_all,
-     q_sems, mate_sems, group_sems, gkv_sems, own_sems) = rest
-    me, mine = lax.axis_index("sp"), lax.axis_index("dp")
-    heads = width // HD
-    length = kv_ref.shape[0]
-    positions = gx_out.shape[0]
-    kv_width = kv_heads * HD
-    per = n // kv_heads
-    plane, member = me // per, lax.rem(me, per)
-    scale = HD ** (-0.5)
-    greet(n, m)
-
-    def target(k):
-        return lax.rem(me + k, n)
-
-    def peer(k):
-        return lax.rem(mine + k, m)
+        kvi_copy(step).wait()
+        start_all(per, lambda k: matei_copy(k, step))
 
     def q_copy(k):
         return remote(
@@ -270,23 +245,34 @@
             def _():
                 q_copy(k).start()
 
-    keys = kv_ref[:, :HD]
-    kt[...] = keys.astype(F32).T.astype(BF16)
-    vs[...] = kv_ref[:, HD:]
-    dk_acc[...] = jnp.zeros_like(dk_acc)
-    dv_acc[...] = jnp.zeros_like(dv_acc)
     lane = lax.broadcasted_iota(jnp.int32, (length, HD), 1)
     ones = jnp.ones((3, length), F32)
     blank = jnp.zeros((HD - 6, length), F32)
+    dk_acc[...] = jnp.zeros_like(dk_acc)
+    dv_acc[...] = jnp.zeros_like(dv_acc)
+    wait_all(n, qi_copy)
     for h in range(heads):
         three = jnp.concatenate(split_bits(gate_ref[h : h + 1, :]), axis=0)
         gates = jnp.concatenate([ones, three, blank, -three, ones, blank], axis=0).T.astype(BF16)
-        q_head = q_ref[:, h * HD : (h + 1) * HD]
-        kx[h] = jnp.concatenate([keys, gates[:, HD:]], axis=1)
+        q_head = q_all[:, h * HD : (h + 1) * HD]
+        kx[h, :, HD:] = gates[:, HD:]
         qx[h] = jnp.concatenate([q_head * jnp.asarray(scale, BF16), gates[:, :HD]], axis=1)
         mark = jnp.where(lane == h, 1.0, 0.0).astype(BF16)
         qd[h] = jnp.concatenate([q_head, mark], axis=1)
-        gh[h] = g_ref[:, h * HD : (h + 1) * HD]
+    wait_all(n, g_copy)
+    for h in range(heads):
+        gh[h] = g_all[:, h * HD : (h + 1) * HD]
+
+    @pl.loop(0, kv_heads)
+    def _(step):
+        wait_all(per, lambda k: matei_copy(k, step))
+
+    wait_all(m, x_copy)
+    keys = kv_all[:, :HD]
+    kt[...] = keys.astype(F32).T.astype(BF16)
+    vs[...] = kv_all[:, HD:]
+    for h in range(heads):
+        kx[h, :, :HD] = keys
     later = lax.broadcasted_iota(jnp.int32, (tile, tile), 0) > lax.broadcasted_iota(
         jnp.int32, (tile, tile), 1
     )
@@ -394,42 +380,74 @@
     )
     gkv_all[mine] = gkv
     start_all(m, gkv_copy)
-    gx_out[...] = dot_nt(gkv, w_ref[...]).astype(BF16)
+    gx_out[...] = dot_nt(gkv, w_all[...]).astype(BF16)
     wait_all(m, gkv_copy)
-    total = dot_tn(x_ref[0], gkv_all[0])
+    total = dot_tn(x_all[0], gkv_all[0])
     for j in range(1, m):
-        total = total + dot_tn(x_ref[j], gkv_all[j])
+        total = total + dot_tn(x_all[j], gkv_all[j])
     share[...] = total.astype(BF16)
     if reduce_here:
-        piece = share.shape[0] // n
+        piece = rows // n
+
+        def rs_mate_copy(k, a):
+            to = lax.rem(member + k, per)
+            return remote(
+                row_block(share, a * per + to, piece), parts.at[member, a],
+                rs_mate_sems.at[a], k, {"sp": plane * per + to},
+            )
 
         def rs_copy(k):
+            a = lax.rem(plane + k, kv_heads)
             return remote(
-                row_block(share, target(k), piece), parts.at[me], rs_sems, k,
-                {"sp": target(k)},
+                rs_sum.at[a], rs_groups.at[plane], rs_sems, k, {"sp": a * per + member}
             )
 
         def ag_copy(k):
-            return remote(
-                mean_block, row_block(whole, me, piece), ag_sems, k, {"sp": target(k)}
-            )
-
-        start_all(n, rs_copy)
-        rs_own = pltpu.make_async_copy(row_block(share, me, piece), parts.at[me], own_sems.at[1])
-        rs_own.start()
-        rs_own.wait()
-        wait_all(n, rs_copy)
-        total = parts[0].astype(F32)
-        for j in range(1, n):
-            total = total + parts[j].astype(F32)
-        mean_block[...] = total.astype(BF16)
-        start_all(n, ag_copy)
-        ag_own = pltpu.make_async_copy(mean_block, row_block(whole, me, piece), own_sems.at[2])
-        ag_own.start()
-        ag_own.wait()
-        wait_all(n, ag_copy)
-        gwk_out[...] = whole[:, :kv_width].astype(F32)
-        gwv_out[...] = whole[:, kv_width:].astype(F32)
+            block = row_block(whole, me, piece)
+            to = lax.rem(plane + k, kv_heads) * per + member
+            return remote(block, block, ag_sems, k, {"sp": to})
+
+        def ag_mate_copy(k, step):
+            source = lax.rem(plane - step + kv_heads, kv_heads) * per + member
+            block = row_block(whole, source, piece)
+            to = plane * per + lax.rem(member + k, per)
+            return remote(block, block, ag_mate_sems.at[step], k, {"sp": to})
+
+        @pl.loop(0, kv_heads)
+        def _(step):
+            start_all(per, lambda k: rs_mate_copy(k, lax.rem(plane + 1 + step, kv_heads)))
+
+        @pl.loop(0, kv_heads)
+        def _(step):
+            a = lax.rem(plane + 1 + step, kv_heads)
+            wait_all(per, lambda k: rs_mate_copy(k, a))
+            total = row_block(share, a * per + member, piece)[...].astype(F32)
+            for k in range(1, per):
+                total = total + parts[lax.rem(member + k, per), a].astype(F32)
+            rs_sum[a] = total.astype(BF16)
+
+            @pl.when(step < kv_heads - 1)
+            def _():
+                rs_copy(step + 1).start()
+
+        total = rs_sum[plane].astype(F32)
+        for k in range(1, kv_heads):
+            rs_copy(k).wait()
+            total = total + rs_groups[lax.rem(plane - k + kv_heads, kv_heads)].astype(F32)
+        row_block(whole, me, piece)[...] = total.astype(BF16)
+        start_all(kv_heads, ag_copy)
+        start_all(per, lambda k: ag_mate_copy(k, 0))
+
+        @pl.loop(1, kv_heads)
+        def _(step):
+            ag_copy(step).wait()
+            start_all(per, lambda k: ag_mate_copy(k, step))
+
+        @pl.loop(0, kv_heads)
+        def _(step):
+            wait_all(per, lambda k: ag_mate_copy(k, step))
+
+        gw_out[...] = whole[...]
     q_own.wait()
     wait_all(n, q_copy)
 
@@ -456,26 +474,6 @@
         if width % LANES == 0:
             return x.reshape(positions, query_width)
         return x.reshape(positions, n, width).transpose(1, 0, 2)
-
-    q_all, g_all, kv_all, w_all, x_all = pl.pallas_call(
-        functools.partial(gather_kernel, n, m, width, kv_heads),
-        out_shape=(
-            shape((length, width)),
-            shape((length, width)),
-            shape((length, 2 * HD)),
-            shape((rows * m, 2 * kv_width)),
-            shape((m, positions, rows)),
-        ),
-        in_specs=[VMEM] * 5,
-        out_specs=(VMEM,) * 5,
-        scratch_shapes=[
-            pltpu.VMEM((positions, 2 * kv_width), BF16),
-            dma((2, n)), dma((2, n)), dma((2, kv_heads)), dma((kv_heads, 2, n // kv_heads)),
-            dma((2, m)), dma((2, m)), dma((2, m)), dma((6,)),
-        ],
-        compiler_params=params(0),
-        name="gather_heads",
-    )(blocks(queries), blocks(cotangent), inputs[0], w_key, w_value)
 
     tile = max(256, positions)
     piece = rows // n
@@ -487,6 +485,14 @@
         shape(gq_shape), shape((positions, feature_count)), shape((heads, length), F32)
     ]
     scratch = [
+        pltpu.VMEM((length, width), BF16),
+        pltpu.VMEM((length, width), BF16),
+        pltpu.VMEM((length, 2 * HD), BF16),
+        pltpu.VMEM((rows * m, 2 * kv_width), BF16),
+        pltpu.VMEM((m, positions, rows), BF16),
+        pltpu.VMEM((positions, 2 * kv_width), BF16),
+        dma((2, n)), dma((2, n)), dma((2, kv_heads)), dma((kv_heads, 2, per)),
+        dma((2, m)), dma((2, m)), dma((2, m)), dma((6,)),
         pltpu.VMEM((heads, length, LANES), BF16),
         pltpu.VMEM((HD, length), BF16),
         pltpu.VMEM((length, HD), BF16),
@@ -503,16 +509,18 @@
         pltpu.VMEM((kv_heads, positions, 2 * HD), BF16),
         pltpu.VMEM((kv_heads, positions, 2 * HD), BF16),
         pltpu.VMEM((m, positions, 2 * kv_width), BF16),
-        dma((2, n)), dma((kv_heads, 2, per)), dma((2, kv_heads)), dma((2, m)), dma((3,)),
+        dma((2, n)), dma((kv_heads, 2, per)), dma((2, kv_heads)), dma((2, m)), dma((1,)),
     ]
     if reduce_here:
-        out_shape += [shape((rows, kv_width), F32)] * 2
+        out_shape += [shape(share_shape)]
         scratch += [
             pltpu.VMEM(share_shape, BF16),
-            pltpu.VMEM((n, piece, 2 * kv_width), BF16),
-            pltpu.VMEM((piece, 2 * kv_width), BF16),
+            pltpu.VMEM((per, kv_heads, piece, 2 * kv_width), BF16),
+            pltpu.VMEM((kv_heads, piece, 2 * kv_width), BF16),
+            pltpu.VMEM((kv_heads, piece, 2 * kv_width), BF16),
             pltpu.VMEM(share_shape, BF16),
-            dma((2, n)), dma((2, n)),
+            dma((kv_heads, 2, per)), dma((2, kv_heads)),
+            dma((2, kv_heads)), dma((kv_heads, 2, per)),
         ]
     else:
         out_shape += [shape(share_shape)]
@@ -522,17 +530,15 @@
         in_specs=[VMEM] * 6,
         out_specs=(VMEM,) * len(out_shape),
         scratch_shapes=scratch,
-        compiler_params=params(1),
+        compiler_params=params(0),
         name="attend_return",
-    )(q_all, g_all, kv_all, cum_gate[0], x_all, w_all)
+    )(blocks(queries), blocks(cotangent), cum_gate[0], inputs[0], w_key, w_value)
     grad_queries, grad_input, grad_cum = results[:3]
     if width % LANES:
         grad_queries = grad_queries.transpose(1, 0, 2)
-    if reduce_here:
-        grad_wk, grad_wv = results[3:]
-    else:
-        summed = lax.psum(results[3], "sp").astype(F32)
-        grad_wk, grad_wv = summed[:, :kv_width], summed[:, kv_width:]
+    summed = results[3] if reduce_here else lax.psum(results[3], "sp")
+    summed = summed.astype(F32)
+    grad_wk, grad_wv = summed[:, :kv_width], summed[:, kv_width:]
     return (
         grad_input.reshape(inputs.shape),
         grad_queries.reshape(queries.shape),

time: 156 us -> 119 us (0.76)
  the two profiles are of different devices: /device:TPU:30 before, /device:TPU:0 now
where the time goes in v2:
time: 119 us; the launch traced here: 118 us
  Pallas kernels  112 us (94%)
  local copies, waits for them, and re-layouts  5.37 us (5%)
    pallas_call x1, Pallas kernels, per_device(): pl.pallas_call(functools.partial(attend_kernel, n, m, width, kv_heads, ti...  112 us
    slice x1, local copies, waits for them, and re-layouts, per_device(): grad_wk, grad_wv = (summed[:, :kv_width], summed[:, kv_width:])  2.74 us
    unnamed x9, local copies, waits for them, and re-layouts  2.64 us

profile of v2, /device:TPU:0, one launch (start us, length us, event | category | flops | bytes accessed | tf_op | source)
XLA Modules:
  0.0 118.4 jit_solution(11719475505150424047)
XLA Ops:
  0.6 112.4 %attend_return.1 = (bf16[128,2048]{1,0:T(8,128)(2,1)}, bf16[128,2048]{1,0:T(8,128)(2,1)}, f32[2,2048]{1,0:T(2,128)}, bf16[1024,512]{1,0:T(8,128)(2,1)}) custom-call(bf16[128,2048]{1,0:T(8,128)(2,1)} %bitcast.7, bf16[128,2048]{1,0:T(8,128)(2,1)} %bitcast.8, f32[2,2048]{1,0:T(2,128)} %bitcast.12, bf16[128,2048]{1,0:T(8,128)(2,1)} %bitcast.9, ...), custom_call_target="tpu_custom_call" | custom-call | tf_op jit(solution)/shard_map/attend_return/pallas_call | solution.py:527
  113.0 0.0 copy-start.1
  113.0 2.7 %fusion = (f32[1024,256]{1,0:T(8,128)}, f32[1024,256]{1,0:T(8,128)}) fusion(bf16[1024,512]{1,0:T(8,128)(2,1)} %get-tuple-element.12), kind=kLoop, calls=%fused_computation | loop fusion | bytes 4194304 | tf_op jit(solution)/shard_map/slice | solution.py:541
  115.8 0.0 copy-done.1
  115.8 0.0 copy-start
  115.8 0.8 copy.14
  116.6 0.4 copy-done
  117.0 0.0 copy-start.2
  117.0 0.8 copy.15
  117.8 0.0 copy-done.2
  117.8 0.6 copy.16
Async XLA Ops:
  113.0 2.7 %copy-start.1 = (bf16[128,2048]{1,0:T(8,128)(2,1)S(1)}, bf16[128,2048]{1,0:T(8,128)(2,1)}, u32[]{:S(2)}) copy-start(bf16[128,2048]{1,0:T(8,128)(2,1)} %get-tuple-element.9) | copy-start | bytes 1572868
  115.8 1.2 %copy-start = (bf16[128,2048]{1,0:T(8,128)(2,1)S(1)}, bf16[128,2048]{1,0:T(8,128)(2,1)}, u32[]{:S(2)}) copy-start(bf16[128,2048]{1,0:T(8,128)(2,1)} %get-tuple-element.10) | copy-start | bytes 1572868
  117.0 0.8 copy-start.2

commit v3 on v2

--- a/solution.py
+++ b/solution.py
@@ -302,6 +302,11 @@
         tops = tuple(jnp.full((8, tile), -jnp.inf, F32) for _ in every)
         tops = lax.fori_loop(0, i, lambda c, v: score(c, v, False), tops)
         tops = score(i, tops, True)
+
+        @pl.when(turn > 0)
+        def _():
+            send_tile(i + 1)
+
         tops = [jnp.max(top, axis=0, keepdims=True) for top in tops]
 
         def weigh(c, carry):
@@ -349,10 +354,6 @@
             [dk_acc[here, :][:, :HD] * scale, dv_acc[here, :]], axis=1
         ).astype(BF16)
 
-        @pl.when(turn > 0)
-        def _():
-            send_tile(i + 1)
-
     send_tile(0)
     q_own.start()
     columns = dk_acc[...].T
@@ -475,7 +476,7 @@
             return x.reshape(positions, query_width)
         return x.reshape(positions, n, width).transpose(1, 0, 2)
 
-    tile = max(256, positions)
+    tile = max(512, positions)
     piece = rows // n
     reduce_here = rows % (16 * n) == 0
     gq_shape = (positions, query_width) if width % LANES == 0 else (n, positions, width)

time: 119 us -> 109 us (0.916)
  Pallas kernels: 112 us -> 103 us
    pallas_call x1, Pallas kernels: 112 us -> 103 us  [per_device(): pl.pallas_call(functools.partial(attend_kernel, n, m, width, kv_heads, ti...]
where the time goes in v3:
time: 109 us
  Pallas kernels  103 us (94%)
  local copies, waits for them, and re-layouts  5.37 us (5%)
    pallas_call x1, Pallas kernels, per_device(): pl.pallas_call(functools.partial(attend_kernel, n, m, width, kv_heads, ti...  103 us
    slice x1, local copies, waits for them, and re-layouts, per_device(): grad_wk, grad_wv = (summed[:, :kv_width], summed[:, kv_width:])  2.74 us
    unnamed x9, local copies, waits for them, and re-layouts  2.64 us

profile of v3, /device:TPU:0, one launch (start us, length us, event | category | flops | bytes accessed | tf_op | source)
XLA Modules:
  0.0 108.6 jit_solution(11266062108538008587)
XLA Ops:
  0.6 102.6 %attend_return.1 = (bf16[128,2048]{1,0:T(8,128)(2,1)}, bf16[128,2048]{1,0:T(8,128)(2,1)}, f32[2,2048]{1,0:T(2,128)}, bf16[1024,512]{1,0:T(8,128)(2,1)}) custom-call(bf16[128,2048]{1,0:T(8,128)(2,1)} %bitcast.7, bf16[128,2048]{1,0:T(8,128)(2,1)} %bitcast.8, f32[2,2048]{1,0:T(2,128)} %bitcast.12, bf16[128,2048]{1,0:T(8,128)(2,1)} %bitcast.9, ...), custom_call_target="tpu_custom_call" | custom-call | tf_op jit(solution)/shard_map/attend_return/pallas_call | solution.py:528
  103.2 0.0 copy-start.1
  103.2 2.7 %fusion = (f32[1024,256]{1,0:T(8,128)}, f32[1024,256]{1,0:T(8,128)}) fusion(bf16[1024,512]{1,0:T(8,128)(2,1)} %get-tuple-element.12), kind=kLoop, calls=%fused_computation | loop fusion | bytes 4194304 | tf_op jit(solution)/shard_map/slice | solution.py:542
  106.0 0.0 copy-done.1
  106.0 0.0 copy-start
  106.0 0.8 copy.14
  106.8 0.4 copy-done
  107.2 0.0 copy-start.2
  107.2 0.8 copy.15
  108.0 0.0 copy-done.2
  108.0 0.6 copy.16
Async XLA Ops:
  103.2 2.7 %copy-start.1 = (bf16[128,2048]{1,0:T(8,128)(2,1)S(1)}, bf16[128,2048]{1,0:T(8,128)(2,1)}, u32[]{:S(2)}) copy-start(bf16[128,2048]{1,0:T(8,128)(2,1)} %get-tuple-element.9) | copy-start | bytes 1572868
  106.0 1.2 %copy-start = (bf16[128,2048]{1,0:T(8,128)(2,1)S(1)}, bf16[128,2048]{1,0:T(8,128)(2,1)}, u32[]{:S(2)}) copy-start(bf16[128,2048]{1,0:T(8,128)(2,1)} %get-tuple-element.10) | copy-start | bytes 1572868
  107.2 0.8 copy-start.2
